TPU v7x, 32 devices: a whole 2x2x4 slice. The times are simulated.
32 devices in a mesh: sp: 8 (over z, y), tp: 4 (over x, core).
Axes of the slice: x: 2, y: 2, z: 4, core: 2. Of those that a mesh axis runs over, the one named last changes fastest.
Arguments:
- residual_in: bfloat16 [3072, 2048], P(('sp', 'tp')), may hold values from -6 to 6
- queries: bfloat16 [3072, 2048], P('sp', 'tp'), may hold values from -180 to 180
- keys: bfloat16 [3072, 2048], P('sp', 'tp'), may hold values from -9 to 9
- values: bfloat16 [3072, 2048], P('sp', 'tp'), may hold values from -6 to 6
- mix_lambda: float32 [16], P('tp'), may hold values from 0.3 to 0.8
- head_gain: float32 [128], replicated, may hold values from 0.1 to 1.9
- out_weight: bfloat16 [2048, 2048], P('tp'), may hold values from -0.125 to 0.125
- norm_gain: float32 [2048], replicated, may hold values from 0.1 to 1.9
- gate_weight: bfloat16 [2048, 5632], P('sp', 'tp'), may hold values from -0.125 to 0.125
- up_weight: bfloat16 [2048, 5632], P('sp', 'tp'), may hold values from -0.125 to 0.125
- down_weight: bfloat16 [5632, 2048], P('tp', 'sp'), may hold values from -0.078125 to 0.078125
Outputs:
- layer_out: bfloat16 [3072, 2048], P(('sp', 'tp'))
All inputs are finite; a program needn't handle non-finite values.
Results may differ from a plain program's by a relative error of at most 0.014.
Values may be sent and summed in bfloat16 or wider, within the bound.
A program may use at most 128 MiB of HBM per device.

v0:
```python
import math
import jax
import jax.numpy as jnp
from jax import lax
from jax.sharding import PartitionSpec as P

DH = 64
VD = 128


def body(
    residual_in,
    queries,
    keys,
    values,
    mix_lambda,
    head_gain,
    out_weight,
    norm_gain,
    gate_weight,
    up_weight,
    down_weight,
):
    tp_count = lax.axis_size("tp")
    tok_local = queries.shape[0]
    heads_local = mix_lambda.shape[0]
    rows_local = tok_local // tp_count
    query_four = queries.reshape(tok_local, heads_local, 2, DH)
    inverse_root = 1.0 / math.sqrt(DH)

    def one_block(state, block):
        top, total, weighted = state
        key_block, value_block = block
        scores = (
            jnp.einsum("qhcd,khcd->hcqk", query_four, key_block, preferred_element_type=jnp.float32)
            * inverse_root
        )
        new_top = jnp.maximum(top, jnp.max(scores, axis=-1))
        rescale = jnp.exp(top - new_top)
        expo = jnp.exp(scores - new_top[..., None])
        total = total * rescale + jnp.sum(expo, axis=-1)
        weighted = weighted * rescale[..., None] + jnp.einsum(
            "hcqk,khe->hcqe",
            expo.astype(jnp.bfloat16),
            value_block,
            preferred_element_type=jnp.float32,
        )
        return ((new_top, total, weighted), None)

    start_state = (
        jnp.full((heads_local, 2, tok_local), -1e30, jnp.float32),
        jnp.zeros((heads_local, 2, tok_local), jnp.float32),
        jnp.zeros((heads_local, 2, tok_local, VD), jnp.float32),
    )
    key_piece = lax.all_gather(keys, "sp", axis=0, tiled=True)
    value_piece = lax.all_gather(values, "sp", axis=0, tiled=True)
    count = key_piece.shape[0]
    shards = max(count // tok_local, 1)
    unit = count // shards
    group = max(
        (g for g in range(1, shards + 1) if shards % g == 0 and g * unit <= max(1536, unit))
    )
    width = group * unit
    blocks = count // width
    key_blocks = key_piece.reshape(blocks, width, heads_local, 2, DH)
    value_blocks = value_piece.reshape(blocks, width, heads_local, VD)
    state, unused = lax.scan(one_block, start_state, (key_blocks, value_blocks))
    top, total, weighted = state
    maps = weighted / total[..., None]
    mixed = maps[:, 0] - mix_lambda[:, None, None] * maps[:, 1]
    head_scale = lax.rsqrt(jnp.mean(mixed * mixed, axis=-1, keepdims=True) + 1e-06)
    head_out = (mixed * head_scale * head_gain).astype(jnp.bfloat16)
    attended = jnp.transpose(head_out, (1, 0, 2)).reshape(tok_local, heads_local * VD)
    summed = lax.psum(
        jnp.dot(attended, out_weight, preferred_element_type=jnp.float32).astype(jnp.bfloat16), "tp"
    ).astype(jnp.float32)
    residual_all = lax.all_gather(residual_in, "tp", axis=0, tiled=True)
    after_all = residual_all.astype(jnp.float32) + summed
    row_scale = lax.rsqrt(jnp.mean(after_all * after_all, axis=-1, keepdims=True) + 1e-06)
    all_rows = (after_all * row_scale * norm_gain).astype(jnp.bfloat16)
    after_mix = lax.dynamic_slice_in_dim(
        after_all, lax.axis_index("tp") * rows_local, rows_local, 0
    )
    gate_all, up_all, down_all = (
        lax.all_gather(gate_weight, "sp", axis=0, tiled=True),
        lax.all_gather(up_weight, "sp", axis=0, tiled=True),
        lax.all_gather(down_weight, "sp", axis=1, tiled=True),
    )
    gate = jnp.dot(all_rows, gate_all, preferred_element_type=jnp.float32)
    up = jnp.dot(all_rows, up_all, preferred_element_type=jnp.float32)
    hidden = (jax.nn.silu(gate) * up).astype(jnp.bfloat16)
    mixer = lax.psum_scatter(
        jnp.dot(hidden, down_all, preferred_element_type=jnp.float32).astype(jnp.bfloat16),
        "tp",
        scatter_dimension=0,
        tiled=True,
    ).astype(jnp.float32)
    return (after_mix + 0.5 * mixer).astype(jnp.bfloat16)


def solution(mesh):
    return jax.shard_map(
        body,
        mesh=mesh,
        in_specs=(
            P(("sp", "tp"), None),
            P("sp", "tp"),
            P("sp", "tp"),
            P("sp", "tp"),
            P("tp"),
            P(),
            P("tp", None),
            P(),
            P("sp", "tp"),
            P("sp", "tp"),
            P("tp", "sp"),
        ),
        out_specs=P(("sp", "tp"), None),
        check_vma=False,
    )
```

profile of v0, /device:TPU:0, one launch (start us, length us, event | category | flops | bytes accessed | tf_op | source)
XLA Modules:
  0.0 579.6 jit_solution(15325134770839630398)
XLA Ops:
  10.0 62.3 %all-gather.9.cloned.1.call-done = bf16[3072,512]{1,0:T(8,128)(2,1)} async-done(((bf16[384,512]{1,0:T(8,128)(2,1)}), bf16[3072,512]{1,0:T(8,128)(2,1)}) %all-gather.9.cloned.1.call-update) | async-done | bytes 3145744 | tf_op jit(solution)/shard_map/all_gather | solution.py:55
  72.3 12.5 %reshape.39 = bf16[2,1536,4,2,64]{4,3,2,1,0:T(2,128)(2,1)} reshape(bf16[3072,512]{1,0:T(8,128)(2,1)} %all-gather.9.cloned.1.call-done) | data formatting | bytes 6291456 | tf_op jit(solution)/shard_map/reshape | solution.py:65
  84.8 15.4 %copy.18 = bf16[2,1536,4,2,64]{1,4,3,2,0:T(8,128)(2,1)} copy(bf16[2,1536,4,2,64]{4,3,2,1,0:T(2,128)(2,1)} %reshape.39) | data formatting | bytes 6291456
  100.2 33.0 %all-gather.11.cloned.1.call-done = bf16[3072,512]{1,0:T(8,128)(2,1)} async-done(((bf16[384,512]{1,0:T(8,128)(2,1)}), bf16[3072,512]{1,0:T(8,128)(2,1)}) %all-gather.11.cloned.1.call-update) | async-done | bytes 3145744 | tf_op jit(solution)/shard_map/all_gather | solution.py:56
  133.2 5.6 reshape.36
  138.7 63.8 %while.15 = (s32[]{:T(128)}, f32[4,2,384]{2,1,0:T(2,128)S(1)}, f32[4,2,384]{2,1,0:T(2,128)S(1)}, f32[4,2,384,128]{3,2,1,0:T(8,128)}, bf16[2,1536,4,2,64]{1,4,3,2...) while((s32[]{:T(128)}, f32[4,2,384]{2,1,0:T(2,128)S(1)}, ...), condition=%wide.region_3.4_spmd.clone, body=%wide.region_0.3_spmd.clone.sunk | while | flops 1850883072 | bytes 79233688 | solution.py:67
  138.7 10.6 %bitcast_reduce_fusion.2 = (f32[4,2,384]{2,1,0:T(2,128)S(1)}, f32[4,2,1536,384]{3,2,1,0:T(8,128)}) fusion(bf16[384,4,2,64]{0,3,2,1:T(8,128)(2,1)S(1)} %get-tuple-element.170, bf16[2,1536,4,2,64]{1,4,3,2,0:T(8,128)(2,1)} %get-tuple-element.169, s32[]{:T(128)} %get-tuple-element.156), kind=kOutput, calls=%fused_computation.1.clone.1 | convolution fusion | flops 613413888 | bytes 20853248 | tf_op jit(solution)/shard_map/while/body/eval_jaxpr/qhcd,khcd->hcqk/dot_general | solution.py:35
  149.4 9.5 %fusion.37 = f32[4,2,384]{2,1,0:T(2,128)S(1)} fusion(f32[4,2,1536,384]{3,2,1,0:T(8,128)} %get-tuple-element.144, f32[4,2,384]{2,1,0:T(2,128)S(1)} %fusion.36), kind=kLoop, calls=%fused_computation.4.clone.1 | loop fusion | flops 14152704 | bytes 18898944 | tf_op jit(solution)/shard_map/while/body/eval_jaxpr/reduce_sum | solution.py:41
  160.7 8.8 %fusion.39 = f32[4,2,384,128]{3,2,1,0:T(8,128)S(1)} fusion(f32[4,2,384,128]{3,2,1,0:T(8,128)S(1)} %copy-done.1, bf16[1,1536,4,128]{3,2,1,0:T(4,128)(2,1)S(1)} %constant_dynamic-slice_fusion.2, f32[4,2,1536,384]{3,2,1,0:T(8,128)} %get-tuple-element.144, f32[4,2,384]{2,1,0:T(2,128)S(1)} %fusion.36, f32[4,2,384]{2,1,0:T(2,128)S(1)} %get-tuple-element.146, ...), kind=kOutput, calls=%fused_computation.12.clone.1 | convolution fusion | flops 1223294976 | bytes 23617536 | tf_op jit(solution)/shard_map/while/body/eval_jaxpr/hcqk,khe->hcqe/dot_general | solution.py:42
  170.7 10.5 %bitcast_reduce_fusion.2 = (f32[4,2,384]{2,1,0:T(2,128)S(1)}, f32[4,2,1536,384]{3,2,1,0:T(8,128)}) fusion(bf16[384,4,2,64]{0,3,2,1:T(8,128)(2,1)S(1)} %get-tuple-element.170, bf16[2,1536,4,2,64]{1,4,3,2,0:T(8,128)(2,1)} %get-tuple-element.169, s32[]{:T(128)} %get-tuple-element.156), kind=kOutput, calls=%fused_computation.1.clone.1 | convolution fusion | flops 613413888 | bytes 20853248 | tf_op jit(solution)/shard_map/while/body/eval_jaxpr/qhcd,khcd->hcqk/dot_general | solution.py:35
  181.2 9.4 %fusion.37 = f32[4,2,384]{2,1,0:T(2,128)S(1)} fusion(f32[4,2,1536,384]{3,2,1,0:T(8,128)} %get-tuple-element.144, f32[4,2,384]{2,1,0:T(2,128)S(1)} %fusion.36), kind=kLoop, calls=%fused_computation.4.clone.1 | loop fusion | flops 14152704 | bytes 18898944 | tf_op jit(solution)/shard_map/while/body/eval_jaxpr/reduce_sum | solution.py:41
  190.7 1.8 constant_dynamic-slice_fusion.2
  192.6 8.8 %fusion.39 = f32[4,2,384,128]{3,2,1,0:T(8,128)S(1)} fusion(f32[4,2,384,128]{3,2,1,0:T(8,128)S(1)} %copy-done.1, bf16[1,1536,4,128]{3,2,1,0:T(4,128)(2,1)S(1)} %constant_dynamic-slice_fusion.2, f32[4,2,1536,384]{3,2,1,0:T(8,128)} %get-tuple-element.144, f32[4,2,384]{2,1,0:T(2,128)S(1)} %fusion.36, f32[4,2,384]{2,1,0:T(2,128)S(1)} %get-tuple-element.146, ...), kind=kOutput, calls=%fused_computation.12.clone.1 | convolution fusion | flops 1223294976 | bytes 23617536 | tf_op jit(solution)/shard_map/while/body/eval_jaxpr/hcqk,khe->hcqe/dot_general | solution.py:42
  202.5 3.1 copy.21
  207.6 2.2 convolution_convert_fusion.1
  211.8 39.7 %all-reduce.2.cloned.1.call-done = bf16[384,2048]{1,0:T(8,128)(2,1)} async-done(((bf16[384,2048]{1,0:T(8,128)(2,1)}), bf16[384,2048]{1,0:T(8,128)(2,1)}) %all-reduce.2.cloned.1.call-update) | async-done | bytes 1572880 | tf_op jit(solution)/shard_map/psum | solution.py:74
  251.5 4.0 convert_add_fusion
  255.5 90.4 %all-gather.13.cloned.1.call-done = bf16[2048,1408]{1,0:T(8,128)(2,1)} async-done(((bf16[256,1408]{1,0:T(8,128)(2,1)}), bf16[2048,1408]{1,0:T(8,128)(2,1)}) %all-gather.13.cloned.1.call-update) | async-done | bytes 5767184 | tf_op jit(solution)/shard_map/all_gather | solution.py:85
  345.9 7.6 %fusion.21 = f32[384,1408]{1,0:T(8,128)} fusion(bf16[2048,1408]{1,0:T(8,128)(2,1)} %all-gather.13.cloned.1.call-done, f32[2048]{0:T(1024)S(1)} %copy-done.5, f32[384]{0:T(512)S(1)} %add_rsqrt_fusion.1, bf16[384,2048]{1,0:T(8,128)(2,1)} %all-reduce.2.cloned.1.call-done, bf16[384,2048]{1,0:T(8,128)(2,1)} %all-gather.7.cloned.1.call-done), kind=kOutput, calls=%fused_computation.40 | convolution fusion | flops 2219311104 | bytes 11085312 | tf_op jit(solution)/shard_map/dot_general | solution.py:89
  353.5 85.0 %all-gather.15.cloned.1.call-done = bf16[2048,1408]{1,0:T(8,128)(2,1)} async-done(((bf16[256,1408]{1,0:T(8,128)(2,1)}), bf16[2048,1408]{1,0:T(8,128)(2,1)}) %all-gather.15.cloned.1.call-update) | async-done | bytes 5767184 | tf_op jit(solution)/shard_map/all_gather | solution.py:86
  438.5 93.4 %all-gather.17.cloned.1.call-done = bf16[1408,2048]{1,0:T(8,128)(2,1)} async-done(((bf16[1408,256]{1,0:T(8,128)(2,1)}), bf16[1408,2048]{1,0:T(8,128)(2,1)}) %all-gather.17.cloned.1.call-update) | async-done | bytes 5767184 | tf_op jit(solution)/shard_map/all_gather | solution.py:87
  531.9 12.4 %convolution_convert_fusion = bf16[384,2048]{1,0:T(8,128)(2,1)} fusion(bf16[1408,2048]{1,0:T(8,128)(2,1)} %all-gather.17.cloned.1.call-done, bf16[2048,1408]{1,0:T(8,128)(2,1)} %all-gather.15.cloned.1.call-done, f32[384,1408]{1,0:T(8,128)} %fusion.21, f32[2048]{0:T(1024)S(1)} %copy-done.5, f32[384]{0:T(512)S(1)} %add_rsqrt_fusion.1, ...), kind=kOutput, calls=%fused_computation.27 | convolution fusion | flops 4437934080 | bytes 18425344 | tf_op jit(solution)/shard_map/dot_general | solution.py:93
  544.3 26.4 %reduce-scatter.2.cloned.1.call-done = bf16[96,2048]{1,0:T(8,128)(2,1)} async-done(((bf16[384,2048]{1,0:T(8,128)(2,1)}), bf16[96,2048]{1,0:T(8,128)(2,1)}) %reduce-scatter.2.cloned.1.call-update) | async-done | bytes 393232 | tf_op jit(solution)/shard_map/reduce_scatter | solution.py:92
  570.7 2.1 add_convert_fusion
  (50 shorter events, 11.6 us)
Async XLA Ops:
  6.5 201.0 %copy-start = (bf16[512,2048]{1,0:T(8,128)(2,1)S(1)}, bf16[512,2048]{1,0:T(8,128)(2,1)}, u32[]{:S(2)}) copy-start(bf16[512,2048]{1,0:T(8,128)(2,1)} %param.19) | copy-start | bytes 6291460
  6.5 65.8 %all-gather.9.cloned.1.call-start = ((), (), s32[]{:S(2)}) async-start(), calls=%async_computation.2 | async-start | bytes 3538944 | tf_op jit(solution)/shard_map/all_gather | solution.py:55
  7.3 125.9 %all-gather.11.cloned.1.call-start = ((), (), s32[]{:S(2)}) async-start(), calls=%async_computation.3 | async-start | bytes 3538944 | tf_op jit(solution)/shard_map/all_gather | solution.py:56
  8.0 203.8 %all-gather.7.cloned.1.call-start = ((), (), s32[]{:S(2)}) async-start(), calls=%async_computation.1 | async-start | bytes 1966080 | tf_op jit(solution)/shard_map/all_gather | solution.py:77
  8.7 242.7 %all-reduce.2.cloned.1.call-start = ((), (), s32[]{:S(2)}) async-start(), calls=%async_computation.4 | async-start | bytes 3145728 | tf_op jit(solution)/shard_map/psum | solution.py:74
  158.8 1.9 copy-start.1
  169.5 1.1 copy-start.2
  190.7 1.9 copy-start.1
  201.3 1.1 copy-start.2
  205.6 1.6 copy-start.3
  205.6 1.8 copy-start.4
  209.8 136.1 %all-gather.13.cloned.1.call-start = ((), (), s32[]{:S(2)}) async-start(), calls=%async_computation.5 | async-start | bytes 6488064 | tf_op jit(solution)/shard_map/all_gather | solution.py:85
  210.4 228.1 %all-gather.15.cloned.1.call-start = ((), (), s32[]{:S(2)}) async-start(), calls=%async_computation.6 | async-start | bytes 6488064 | tf_op jit(solution)/shard_map/all_gather | solution.py:86
  210.9 321.0 %all-gather.17.cloned.1.call-start = ((), (), s32[]{:S(2)}) async-start(), calls=%async_computation.7 | async-start | bytes 6488064 | tf_op jit(solution)/shard_map/all_gather | solution.py:87
  211.7 134.2 %copy-start.5 = (f32[2048]{0:T(1024)S(1)}, f32[2048]{0:T(1024)}, u32[]{:S(2)}) copy-start(f32[2048]{0:T(1024)} %param.20) | copy-start | bytes 24580
  211.7 359.0 %reduce-scatter.2.cloned.1.call-start = ((), (), s32[]{:S(2)}) async-start(), calls=%async_computation.8 | async-start | bytes 1966080 | tf_op jit(solution)/shard_map/reduce_scatter | solution.py:92
Sparse Core Ops, SparseCore 0:
  9.5 62.7 all-gather.8
  74.5 58.6 all-gather.10
  134.7 18.2 all-gather.6
  209.9 41.5 all-reduce.1
  253.5 92.3 all-gather.12
  347.9 90.5 all-gather.14
  440.5 91.2 all-gather.16
  544.4 26.2 reduce-scatter.1
where the time goes:
time: 581 us; the launch traced here: 580 us
  waiting for transfers between devices  434 us (75%)
  matrix products  60.9 us (10%)
  local copies, waits for them, and re-layouts  43.7 us (8%)
  other arithmetic  27.1 us (5%)
  between operations  13.6 us (2%)
    all_gather x1, waiting for transfers between devices, body(): lax.all_gather(down_weight, 'sp', axis=1, tiled=True)  93.4 us
    all_gather x1, waiting for transfers between devices, body(): lax.all_gather(gate_weight, 'sp', axis=0, tiled=True)  90.4 us
    all_gather x1, waiting for transfers between devices, body(): lax.all_gather(up_weight, 'sp', axis=0, tiled=True)  85 us
    all_gather x1, waiting for transfers between devices, body(): key_piece = lax.all_gather(keys, 'sp', axis=0, tiled=True)  62.3 us
    psum x1, waiting for transfers between devices, body(): lax.psum(jnp.dot(attended, out_weight, preferred_element_type=jnp.float32...  39.7 us
    all_gather x1, waiting for transfers between devices, body(): value_piece = lax.all_gather(values, 'sp', axis=0, tiled=True)  33 us
    reduce_scatter x1, waiting for transfers between devices, body(): lax.psum_scatter(jnp.dot(hidden, down_all, preferred_element_type=jnp.flo...  26.4 us
    dot_general x2, matrix products, one_block(): jnp.einsum('qhcd,khcd->hcqk', query_four, key_block, preferred_element_ty...  21.1 us
  transfers between devices with their start and end apart: 8, of which 7 were waited for; matrix products, arithmetic and copies ran while one was open for 20% of the time, Pallas kernels for 0%

commit v1 on v0

--- a/solution.py
+++ b/solution.py
@@ -84,7 +84,9 @@
     gate_all, up_all, down_all = (
         lax.all_gather(gate_weight, "sp", axis=0, tiled=True),
         lax.all_gather(up_weight, "sp", axis=0, tiled=True),
-        lax.all_gather(down_weight, "sp", axis=1, tiled=True),
+        jnp.concatenate(
+            lax.all_to_all(jnp.stack([down_weight] * lax.axis_size("sp")), "sp", 0, 0), axis=1
+        ),
     )
     gate = jnp.dot(all_rows, gate_all, preferred_element_type=jnp.float32)
     up = jnp.dot(all_rows, up_all, preferred_element_type=jnp.float32)

time: 581 us -> 557 us (0.959)
  waiting for transfers between devices: 434 us -> 402 us
    all_gather x1 -> x0, waiting for transfers between devices: 93.4 us -> none  [body(): lax.all_gather(down_weight, 'sp', axis=1, tiled=True)]
    all_gather x1, waiting for transfers between devices: 90.4 us -> 159 us  [body(): lax.all_gather(gate_weight, 'sp', axis=0, tiled=True)]
    psum x1, waiting for transfers between devices: 39.7 us -> 32 us  [body(): lax.psum(jnp.dot(attended, out_weight, preferred_element_type=jnp.float32...]
    unnamed x10 -> x13, local copies, waits for them, and re-layouts: 16.7 us -> 17.5 us
  transfers between devices with their start and end apart: 8 -> 8, of which waited for: 7 -> 6; matrix products, arithmetic and copies ran while one was open for 20% -> 21% of each run, Pallas kernels for 0% -> 0%
where the time goes in v1:
time: 557 us; the launch traced here: 556 us
  waiting for transfers between devices  402 us (72%)
  matrix products  60.8 us (11%)
  local copies, waits for them, and re-layouts  47.6 us (9%)
  other arithmetic  27.2 us (5%)
  between operations  13.6 us (2%)
    all_gather x1, waiting for transfers between devices, body(): lax.all_gather(gate_weight, 'sp', axis=0, tiled=True)  159 us
    all_gather x1, waiting for transfers between devices, body(): lax.all_gather(up_weight, 'sp', axis=0, tiled=True)  85.5 us
    all_gather x1, waiting for transfers between devices, body(): key_piece = lax.all_gather(keys, 'sp', axis=0, tiled=True)  62.3 us
    all_gather x1, waiting for transfers between devices, body(): value_piece = lax.all_gather(values, 'sp', axis=0, tiled=True)  33 us
    psum x1, waiting for transfers between devices, body(): lax.psum(jnp.dot(attended, out_weight, preferred_element_type=jnp.float32...  32 us
    reduce_scatter x1, waiting for transfers between devices, body(): lax.psum_scatter(jnp.dot(hidden, down_all, preferred_element_type=jnp.flo...  26.4 us
    dot_general x2, matrix products, one_block(): jnp.einsum('qhcd,khcd->hcqk', query_four, key_block, preferred_element_ty...  21.1 us
    reduce_sum x2, other arithmetic, one_block(): total = total * rescale + jnp.sum(expo, axis=-1)  18.9 us
  transfers between devices with their start and end apart: 8, of which 6 were waited for; matrix products, arithmetic and copies ran while one was open for 21% of the time, Pallas kernels for 0%

profile of v1, /device:TPU:0, one launch (start us, length us, event | category | flops | bytes accessed | tf_op | source)
XLA Modules:
  0.0 555.7 jit_solution(18149851041746697276)
XLA Ops:
  10.0 62.3 %all-gather.8.cloned.1.call-done = bf16[3072,512]{1,0:T(8,128)(2,1)} async-done(((bf16[384,512]{1,0:T(8,128)(2,1)}), bf16[3072,512]{1,0:T(8,128)(2,1)}) %all-gather.8.cloned.1.call-update) | async-done | bytes 3145744 | tf_op jit(solution)/shard_map/all_gather | solution.py:55
  72.3 12.5 %reshape.49 = bf16[2,1536,4,2,64]{4,3,2,1,0:T(2,128)(2,1)} reshape(bf16[3072,512]{1,0:T(8,128)(2,1)} %all-gather.8.cloned.1.call-done) | data formatting | bytes 6291456 | tf_op jit(solution)/shard_map/reshape | solution.py:65
  84.8 15.4 %copy.18 = bf16[2,1536,4,2,64]{1,4,3,2,0:T(8,128)(2,1)} copy(bf16[2,1536,4,2,64]{4,3,2,1,0:T(2,128)(2,1)} %reshape.49) | data formatting | bytes 6291456
  100.2 33.0 %all-gather.10.cloned.1.call-done = bf16[3072,512]{1,0:T(8,128)(2,1)} async-done(((bf16[384,512]{1,0:T(8,128)(2,1)}), bf16[3072,512]{1,0:T(8,128)(2,1)}) %all-gather.10.cloned.1.call-update) | async-done | bytes 3145744 | tf_op jit(solution)/shard_map/all_gather | solution.py:56
  133.2 5.6 %reshape.44 = bf16[2,1536,4,128]{3,2,1,0:T(4,128)(2,1)} reshape(bf16[3072,512]{1,0:T(8,128)(2,1)} %all-gather.10.cloned.1.call-done) | data formatting | bytes 6291456 | tf_op jit(solution)/shard_map/reshape | solution.py:66
  138.7 63.9 %while.15 = (s32[]{:T(128)}, f32[4,2,384]{2,1,0:T(2,128)S(1)}, f32[4,2,384]{2,1,0:T(2,128)S(1)}, f32[4,2,384,128]{3,2,1,0:T(8,128)}, bf16[2,1536,4,2,64]{1,4,3,2...) while((s32[]{:T(128)}, f32[4,2,384]{2,1,0:T(2,128)S(1)}, ...), condition=%wide.region_3.4_spmd.clone, body=%wide.region_0.3_spmd.clone.sunk | while | flops 1850883072 | bytes 79233688 | solution.py:67
  138.7 10.6 %bitcast_reduce_fusion.2 = (f32[4,2,384]{2,1,0:T(2,128)S(1)}, f32[4,2,1536,384]{3,2,1,0:T(8,128)}) fusion(bf16[384,4,2,64]{0,3,2,1:T(8,128)(2,1)S(1)} %get-tuple-element.170, bf16[2,1536,4,2,64]{1,4,3,2,0:T(8,128)(2,1)} %get-tuple-element.169, s32[]{:T(128)} %get-tuple-element.156), kind=kOutput, calls=%fused_computation.1.clone.1 | convolution fusion | flops 613413888 | bytes 20853248 | tf_op jit(solution)/shard_map/while/body/eval_jaxpr/qhcd,khcd->hcqk/dot_general | solution.py:35
  149.4 9.5 %fusion.37 = f32[4,2,384]{2,1,0:T(2,128)S(1)} fusion(f32[4,2,1536,384]{3,2,1,0:T(8,128)} %get-tuple-element.144, f32[4,2,384]{2,1,0:T(2,128)S(1)} %fusion.36), kind=kLoop, calls=%fused_computation.4.clone.1 | loop fusion | flops 14152704 | bytes 18898944 | tf_op jit(solution)/shard_map/while/body/eval_jaxpr/reduce_sum | solution.py:41
  160.7 8.8 %fusion.39 = f32[4,2,384,128]{3,2,1,0:T(8,128)S(1)} fusion(f32[4,2,384,128]{3,2,1,0:T(8,128)S(1)} %copy-done.1, bf16[1,1536,4,128]{3,2,1,0:T(4,128)(2,1)S(1)} %constant_dynamic-slice_fusion.2, f32[4,2,1536,384]{3,2,1,0:T(8,128)} %get-tuple-element.144, f32[4,2,384]{2,1,0:T(2,128)S(1)} %fusion.36, f32[4,2,384]{2,1,0:T(2,128)S(1)} %get-tuple-element.146, ...), kind=kOutput, calls=%fused_computation.12.clone.1 | convolution fusion | flops 1223294976 | bytes 23617536 | tf_op jit(solution)/shard_map/while/body/eval_jaxpr/hcqk,khe->hcqe/dot_general | solution.py:42
  170.7 10.5 %bitcast_reduce_fusion.2 = (f32[4,2,384]{2,1,0:T(2,128)S(1)}, f32[4,2,1536,384]{3,2,1,0:T(8,128)}) fusion(bf16[384,4,2,64]{0,3,2,1:T(8,128)(2,1)S(1)} %get-tuple-element.170, bf16[2,1536,4,2,64]{1,4,3,2,0:T(8,128)(2,1)} %get-tuple-element.169, s32[]{:T(128)} %get-tuple-element.156), kind=kOutput, calls=%fused_computation.1.clone.1 | convolution fusion | flops 613413888 | bytes 20853248 | tf_op jit(solution)/shard_map/while/body/eval_jaxpr/qhcd,khcd->hcqk/dot_general | solution.py:35
  181.3 9.4 %fusion.37 = f32[4,2,384]{2,1,0:T(2,128)S(1)} fusion(f32[4,2,1536,384]{3,2,1,0:T(8,128)} %get-tuple-element.144, f32[4,2,384]{2,1,0:T(2,128)S(1)} %fusion.36), kind=kLoop, calls=%fused_computation.4.clone.1 | loop fusion | flops 14152704 | bytes 18898944 | tf_op jit(solution)/shard_map/while/body/eval_jaxpr/reduce_sum | solution.py:41
  192.6 8.8 %fusion.39 = f32[4,2,384,128]{3,2,1,0:T(8,128)S(1)} fusion(f32[4,2,384,128]{3,2,1,0:T(8,128)S(1)} %copy-done.1, bf16[1,1536,4,128]{3,2,1,0:T(4,128)(2,1)S(1)} %constant_dynamic-slice_fusion.2, f32[4,2,1536,384]{3,2,1,0:T(8,128)} %get-tuple-element.144, f32[4,2,384]{2,1,0:T(2,128)S(1)} %fusion.36, f32[4,2,384]{2,1,0:T(2,128)S(1)} %get-tuple-element.146, ...), kind=kOutput, calls=%fused_computation.12.clone.1 | convolution fusion | flops 1223294976 | bytes 23617536 | tf_op jit(solution)/shard_map/while/body/eval_jaxpr/hcqk,khe->hcqe/dot_general | solution.py:42
  202.6 3.0 copy.21
  207.6 2.2 convolution_convert_fusion.1
  211.3 2.9 stack.2
  214.2 4.7 all-to-all-start
  219.6 32.0 %all-reduce.2.cloned.1.call-done = bf16[384,2048]{1,0:T(8,128)(2,1)} async-done(((bf16[384,2048]{1,0:T(8,128)(2,1)}), bf16[384,2048]{1,0:T(8,128)(2,1)}) %all-reduce.2.cloned.1.call-update) | async-done | bytes 1572880 | tf_op jit(solution)/shard_map/psum | solution.py:74
  251.5 4.1 convert_add_fusion
  255.6 159.3 %all-gather.12.cloned.1.call-done = bf16[2048,1408]{1,0:T(8,128)(2,1)} async-done(((bf16[256,1408]{1,0:T(8,128)(2,1)}), bf16[2048,1408]{1,0:T(8,128)(2,1)}) %all-gather.12.cloned.1.call-update) | async-done | bytes 5767184 | tf_op jit(solution)/shard_map/all_gather | solution.py:85
  414.9 7.7 %fusion.21 = f32[384,1408]{1,0:T(8,128)} fusion(bf16[2048,1408]{1,0:T(8,128)(2,1)} %all-gather.12.cloned.1.call-done, f32[2048]{0:T(1024)S(1)} %copy-done.6, f32[384]{0:T(512)S(1)} %add_rsqrt_fusion.1, bf16[384,2048]{1,0:T(8,128)(2,1)} %all-reduce.2.cloned.1.call-done, bf16[384,2048]{1,0:T(8,128)(2,1)} %all-gather.6.cloned.1.call-done), kind=kOutput, calls=%fused_computation.40 | convolution fusion | flops 2219311104 | bytes 11085312 | tf_op jit(solution)/shard_map/dot_general | solution.py:91
  422.6 85.5 %all-gather.14.cloned.1.call-done = bf16[2048,1408]{1,0:T(8,128)(2,1)} async-done(((bf16[256,1408]{1,0:T(8,128)(2,1)}), bf16[2048,1408]{1,0:T(8,128)(2,1)}) %all-gather.14.cloned.1.call-update) | async-done | bytes 5767184 | tf_op jit(solution)/shard_map/all_gather | solution.py:86
  508.1 12.2 %convolution_convert_fusion = bf16[384,2048]{1,0:T(8,128)(2,1)} fusion(bf16[1408,2048]{0,1:T(8,128)(2,1)} %bitcast.6, bf16[2048,1408]{1,0:T(8,128)(2,1)} %all-gather.14.cloned.1.call-done, f32[384,1408]{1,0:T(8,128)} %fusion.21, f32[2048]{0:T(1024)S(1)} %copy-done.6, f32[384]{0:T(512)S(1)} %add_rsqrt_fusion.1, ...), kind=kOutput, calls=%fused_computation.27 | convolution fusion | flops 4437934080 | bytes 18425344 | tf_op jit(solution)/shard_map/dot_general | solution.py:95
  520.4 26.4 %reduce-scatter.2.cloned.1.call-done = bf16[96,2048]{1,0:T(8,128)(2,1)} async-done(((bf16[384,2048]{1,0:T(8,128)(2,1)}), bf16[96,2048]{1,0:T(8,128)(2,1)}) %reduce-scatter.2.cloned.1.call-update) | async-done | bytes 393232 | tf_op jit(solution)/shard_map/reduce_scatter | solution.py:94
  546.8 2.1 add_convert_fusion
  (53 shorter events, 13.6 us)
Async XLA Ops:
  6.5 201.1 %copy-start = (bf16[512,2048]{1,0:T(8,128)(2,1)S(1)}, bf16[512,2048]{1,0:T(8,128)(2,1)}, u32[]{:S(2)}) copy-start(bf16[512,2048]{1,0:T(8,128)(2,1)} %param.19) | copy-start | bytes 6291460
  6.5 65.8 %all-gather.8.cloned.1.call-start = ((), (), s32[]{:S(2)}) async-start(), calls=%async_computation.3 | async-start | bytes 3538944 | tf_op jit(solution)/shard_map/all_gather | solution.py:55
  7.3 125.9 %all-gather.10.cloned.1.call-start = ((), (), s32[]{:S(2)}) async-start(), calls=%async_computation.4 | async-start | bytes 3538944 | tf_op jit(solution)/shard_map/all_gather | solution.py:56
  8.0 211.6 %all-gather.6.cloned.1.call-start = ((), (), s32[]{:S(2)}) async-start(), calls=%async_computation.2 | async-start | bytes 1966080 | tf_op jit(solution)/shard_map/all_gather | solution.py:77
  8.7 242.8 %all-reduce.2.cloned.1.call-start = ((), (), s32[]{:S(2)}) async-start(), calls=%async_computation.5 | async-start | bytes 3145728 | tf_op jit(solution)/shard_map/psum | solution.py:74
  158.8 1.9 copy-start.1
  169.5 1.2 copy-start.2
  190.7 1.9 copy-start.1
  201.4 1.2 copy-start.2
  205.6 1.6 copy-start.4
  205.6 1.8 copy-start.5
  209.8 1.1 copy-start.3
  209.8 205.1 %all-gather.12.cloned.1.call-start = ((), (), s32[]{:S(2)}) async-start(), calls=%async_computation.6 | async-start | bytes 6488064 | tf_op jit(solution)/shard_map/all_gather | solution.py:85
  214.2 208.4 %all-to-all-start = ((bf16[8,1408,256]{1,2,0:T(8,128)(2,1)}), bf16[8,1408,256]{1,2,0:T(8,128)(2,1)}, u32[]{:S(2)}, u32[]{:S(2)}) async-start(bf16[8,1408,256]{1,2,0:T(8,128)(2,1)} %stack.2), calls=%async_computation | async-start | bytes 11534336 | tf_op jit(solution)/shard_map/all_to_all | solution.py:88
  218.9 289.2 %all-gather.14.cloned.1.call-start = ((), (), s32[]{:S(2)}) async-start(), calls=%async_computation.7 | async-start | bytes 6488064 | tf_op jit(solution)/shard_map/all_gather | solution.py:86
  219.5 195.4 %copy-start.6 = (f32[2048]{0:T(1024)S(1)}, f32[2048]{0:T(1024)}, u32[]{:S(2)}) copy-start(f32[2048]{0:T(1024)} %param.20) | copy-start | bytes 24580
  219.5 327.3 %reduce-scatter.2.cloned.1.call-start = ((), (), s32[]{:S(2)}) async-start(), calls=%async_computation.8 | async-start | bytes 1966080 | tf_op jit(solution)/shard_map/reduce_scatter | solution.py:94
Sparse Core Ops, SparseCore 0:
  9.5 62.7 all-gather.7
  74.5 58.6 all-gather.9
  134.7 18.2 all-gather.5
  210.0 41.5 all-reduce.1
  253.6 161.2 all-gather.11
  416.9 91.1 all-gather.13
  520.5 26.2 reduce-scatter.1
